TPU v7x, 32 devices: a whole 2x2x4 slice. The times are simulated.
32 devices in a mesh: kv: 8 (over z, x), tp: 4 (over y, core).
Axes of the slice: x: 2, y: 2, z: 4, core: 2. Of those that a mesh axis runs over, the one named last changes fastest.
Arguments:
- tokens: bfloat16 [288, 4096], P(None, 'kv'), may hold values from -40 to 40
- norm_gain: float32 [4096], P('kv'), may hold values from 0.1 to 1.9
- query_weight: bfloat16 [4096, 2048], P('kv', 'tp'), may hold values from -0.09375 to 0.09375
- key_weight: bfloat16 [4096, 2048], P('kv', 'tp'), may hold values from -0.09375 to 0.09375
- value_weight: bfloat16 [4096, 2048], P('kv', 'tp'), may hold values from -0.09375 to 0.09375
- gate_weight: bfloat16 [4096, 32], replicated, may hold values from -0.09375 to 0.09375
- gate_bias: float32 [32], replicated, may hold values from -0.5 to 3
- out_weight: bfloat16 [2048, 4096], P('tp', 'kv'), may hold values from -0.125 to 0.125
- cache_keys: bfloat16 [12, 3072, 2048], P(None, 'kv', 'tp'), may hold values from -1000 to 1000
- cache_values: bfloat16 [12, 3072, 2048], P(None, 'kv', 'tp'), may hold values from -6 to 6
- cache_decay: float32 [12, 32, 3072], P(None, 'tp', 'kv'), may hold values from -3072 to 0, as said below
- lengths: int32 [12], replicated, may hold values from 1537 to 3072
- parents: int32 [12, 24], replicated, may hold values from 0 to 23, as said below
Outputs:
- mixed: bfloat16 [288, 4096], P('tp', 'kv')
Inputs may be any that keep to these rules, and one draw needn't show every extreme that they name: `cache_decay`: zero at and beyond lengths of the sequence. parents[s, 0] = 0 and parents[s, n] < n for n > 0.
All inputs are finite; a program needn't handle non-finite values.
Results may differ from a plain program's by a relative error of at most 0.014.
The roundings to bfloat16 on the way count: a program that leaves them out, or rounds other values in their place, can miss the bound.
Values may be sent and summed in bfloat16 or wider, within the bound.
A program may use at most 64 MiB of HBM per device.

v0:
```python
import jax
import jax.numpy as jnp
from jax import lax
from jax.sharding import PartitionSpec as P


def ancestry_of(parents):
    count = parents.shape[1]
    nodes = jnp.arange(count, dtype=jnp.int32)
    link = (parents[:, :, None] == nodes[None, None, :]).astype(jnp.float32)
    link = jnp.maximum(link, jnp.eye(count, dtype=jnp.float32)[None])
    for _ in range(count.bit_length()):
        link = jnp.minimum(
            jnp.einsum("snm,smk->snk", link, link, precision=lax.Precision.HIGHEST), 1.0
        )
    return link


def finish(cache_top, cache_total, cache_mix, tree_top, tree_total, tree_mix):
    top = jnp.maximum(cache_top, tree_top)
    cache_factor = jnp.exp(cache_top - top)
    tree_factor = jnp.exp(tree_top - top)
    numer = cache_factor[..., None] * cache_mix + tree_factor[..., None] * tree_mix
    denom = cache_factor * cache_total + tree_factor * tree_total
    return (numer / denom[..., None]).astype(jnp.bfloat16)


def body(
    tokens,
    norm_gain,
    query_weight,
    key_weight,
    value_weight,
    gate_weight,
    gate_bias,
    out_weight,
    cache_keys,
    cache_values,
    cache_decay,
    lengths,
    parents,
):
    rows, width_dev = tokens.shape
    seqs, props = parents.shape
    heads_dev = cache_decay.shape[1]
    pos_dev = cache_keys.shape[1]
    head_dim = query_weight.shape[1] // heads_dev
    scale = head_dim ** (-0.5)
    kv_index = lax.axis_index("kv")
    tp_index = lax.axis_index("tp")
    full_width = width_dev * lax.axis_size("kv")
    xf = tokens.astype(jnp.float32)
    squares = jnp.sum(xf * xf, axis=1)
    normed = (xf * norm_gain).astype(jnp.bfloat16)
    gate_rows = lax.dynamic_slice_in_dim(gate_weight, kv_index * width_dev, width_dev, 0)
    stacked = jnp.stack(
        [
            jnp.dot(normed, weight, preferred_element_type=jnp.float32)
            for weight in (query_weight, key_weight, value_weight)
        ],
        axis=1,
    )
    gate_part = jnp.dot(normed, gate_rows, preferred_element_type=jnp.float32)
    stacked, gate_part, squares = lax.psum((stacked, gate_part, squares), "kv")
    inverse = lax.rsqrt(squares / full_width + 1e-06)[:, None]
    fresh = (inverse[:, :, None] * stacked).astype(jnp.bfloat16)
    log_gates = jax.nn.log_sigmoid(inverse * gate_part + gate_bias)
    own_gates = lax.dynamic_slice_in_dim(log_gates, tp_index * heads_dev, heads_dev, 1).reshape(
        seqs, props, heads_dev
    )
    queries = fresh[:, 0].reshape(seqs, props, heads_dev, head_dim)
    new_keys = fresh[:, 1].reshape(seqs, props, heads_dev, head_dim)
    new_values = fresh[:, 2].reshape(seqs, props, heads_dev, head_dim)
    ancestry = ancestry_of(parents)
    path = jnp.einsum("snk,skh->snh", ancestry, own_gates, precision=lax.Precision.HIGHEST)
    keys = cache_keys.reshape(seqs, pos_dev, heads_dev, head_dim)
    values = cache_values.reshape(seqs, pos_dev, heads_dev, head_dim)
    scores = (
        jnp.einsum("snhd,sjhd->snhj", queries, keys, preferred_element_type=jnp.float32) * scale
    )
    scores = scores + path[..., None] + cache_decay[:, None, :, :]
    position = kv_index * pos_dev + jnp.arange(pos_dev, dtype=jnp.int32)
    live = (position[None, :] < lengths[:, None])[:, None, None, :]
    scores = jnp.where(live, scores, -1e30)
    cache_top = jnp.max(scores, axis=-1)
    weights = jnp.where(live, jnp.exp(scores - cache_top[..., None]), 0.0)
    cache_total = jnp.sum(weights, axis=-1).reshape(rows, heads_dev)
    cache_mix = jnp.einsum(
        "snhj,sjhd->snhd", weights.astype(jnp.bfloat16), values, preferred_element_type=jnp.float32
    ).reshape(rows, heads_dev, head_dim)
    cache_top = cache_top.reshape(rows, heads_dev)
    tree_scores = (
        jnp.einsum("snhd,skhd->snhk", queries, new_keys, preferred_element_type=jnp.float32) * scale
    )
    tree_scores = tree_scores + path[..., None] - jnp.swapaxes(path, 1, 2)[:, None, :, :]
    tree_live = ancestry[:, :, None, :] > 0.5
    tree_scores = jnp.where(tree_live, tree_scores, -1e30)
    tree_top = jnp.max(tree_scores, axis=-1)
    tree_weights = jnp.where(tree_live, jnp.exp(tree_scores - tree_top[..., None]), 0.0)
    tree_total = jnp.sum(tree_weights, axis=-1).reshape(rows, heads_dev)
    tree_mix = jnp.einsum(
        "snhk,skhd->snhd",
        tree_weights.astype(jnp.bfloat16),
        new_values,
        preferred_element_type=jnp.float32,
    ).reshape(rows, heads_dev, head_dim)
    tree_top = tree_top.reshape(rows, heads_dev)
    block = rows // lax.axis_size("kv")
    tops, totals, mixes = (
        lax.all_to_all(cache_top[None], "kv", split_axis=1, concat_axis=0, tiled=True),
        lax.all_to_all(cache_total[None], "kv", split_axis=1, concat_axis=0, tiled=True),
        lax.all_to_all(cache_mix[None], "kv", split_axis=1, concat_axis=0, tiled=True),
    )
    best = jnp.max(tops, axis=0)
    factors = jnp.exp(tops - best[None])
    merged_total = jnp.sum(factors * totals, axis=0)
    merged_mix = jnp.sum(factors[..., None] * mixes, axis=0)
    start = kv_index * block
    piece = finish(
        best,
        merged_total,
        merged_mix,
        lax.dynamic_slice_in_dim(tree_top, start, block, 0),
        lax.dynamic_slice_in_dim(tree_total, start, block, 0),
        lax.dynamic_slice_in_dim(tree_mix, start, block, 0),
    )
    attended = lax.all_gather(piece.reshape(block, heads_dev * head_dim), "kv", axis=0, tiled=True)
    term = jnp.dot(attended, out_weight, preferred_element_type=jnp.float32)
    return lax.psum_scatter(term.astype(jnp.bfloat16), "tp", scatter_dimension=0, tiled=True)


def solution(mesh):
    in_specs = (
        P(None, "kv"),
        P("kv"),
        P("kv", "tp"),
        P("kv", "tp"),
        P("kv", "tp"),
        P(),
        P(),
        P("tp", "kv"),
        P(None, "kv", "tp"),
        P(None, "kv", "tp"),
        P(None, "tp", "kv"),
        P(),
        P(),
    )
    out_specs = P("tp", "kv")
    return jax.shard_map(body, mesh=mesh, in_specs=in_specs, out_specs=out_specs, check_vma=False)
```

profile of v0, /device:TPU:0, one launch (start us, length us, event | category | flops | bytes accessed | tf_op | source)
XLA Modules:
  0.0 231.3 jit_solution(12476319667782251723)
XLA Ops:
  7.7 1.3 convolution_bitcast_fusion.3
  9.0 1.3 convolution_bitcast_fusion.2
  10.7 1.4 pad_maximum_fusion
  13.2 41.0 %all-reduce = (f32[288]{0:T(512)S(1)}, f32[288,32]{0,1:T(8,128)S(1)}) all-reduce(f32[288]{0:T(512)S(1)} %fusion.18, f32[288,32]{0,1:T(8,128)S(1)} %fusion.28), channel_id=1, replica_groups=mesh['kv'=8,'tp'=4] {'kv'}, use_global_device_ids=true, to_apply=%region_1.0 | all-reduce | flops 9504 | bytes 76032 | tf_op jit(solution)/shard_map/psum | solution.py:64
  54.5 6.6 %copy.56 = bf16[12,384,512]{1,2,0:T(8,128)(2,1)} copy(bf16[12,384,512]{2,1,0:T(8,128)(2,1)} %param.21) | data formatting | bytes 9437184 | tf_op args[8]
  63.6 45.9 %all-reduce.3.cloned.1.call-done = f32[288,3,512]{2,0,1:T(8,128)} async-done(((f32[288,3,512]{2,0,1:T(8,128)}), f32[288,3,512]{2,0,1:T(8,128)}) %all-reduce.3.cloned.1.call-update) | async-done | bytes 1769488 | tf_op jit(solution)/shard_map/psum | solution.py:64
  109.5 1.6 multiply_convert_fusion
  112.3 3.2 %fusion.55 = (f32[12,24,8]{1,2,0:T(8,128)S(1)}, f32[12,24,8,384]{3,1,2,0:T(8,128)S(1)}) fusion(f32[12,8,384]{2,1,0:T(8,128)S(1)} %copy-done.8, f32[12,24,8]{1,2,0:T(8,128)S(1)} %fusion.37, bf16[12,384,8,64]{1,3,2,0:T(8,128)(2,1)} %bitcast.72, bf16[12,24,8,64]{3,2,1,0:T(8,128)(2,1)S(1)} %reshape_squeeze.9, pred[12,384]{1,0:T(8,128)(4,1)S(1)} %broadcast_compare_fusion.1), kind=kOutput, calls=%fused_computation.79 | convolution fusion | flops 117667584 | bytes 8722944 | tf_op jit(solution)/shard_map/snhd,sjhd->snhj/dot_general | solution.py:79
  115.6 1.7 copy-done.1
  117.3 1.2 fusion.2
  120.7 4.0 %all-to-all-start.2 = ((f32[8,1,288]{2,1,0:T(1,128)}), f32[8,1,288]{2,1,0:T(1,128)S(1)}, u32[]{:S(2)}, u32[]{:S(2)}) async-start(f32[8,1,288]{2,1,0:T(1,128)} %reshape.107), calls=%async_computation.2 | async-start | bytes 24576 | tf_op jit(solution)/shard_map/all_to_all | solution.py:111
  125.5 6.6 %copy.68 = bf16[12,384,512]{1,2,0:T(8,128)(2,1)} copy(bf16[12,384,512]{2,1,0:T(8,128)(2,1)} %param.22) | data formatting | bytes 9437184 | tf_op args[9]
  133.8 6.0 %all-to-all-start = ((f32[8,1,288]{2,1,0:T(1,128)}), f32[8,1,288]{2,1,0:T(1,128)S(1)}, u32[]{:S(2)}, u32[]{:S(2)}) async-start(f32[8,1,288]{2,1,0:T(1,128)} %reshape.105), calls=%async_computation | async-start | bytes 24576 | tf_op jit(solution)/shard_map/all_to_all | solution.py:110
  139.8 5.2 %fusion.9 = f32[12,24,8,64]{3,1,2,0:T(8,128)S(1)} fusion(bf16[12,384,8,64]{1,3,2,0:T(8,128)(2,1)} %bitcast.73, f32[12,24,8,384]{3,1,2,0:T(8,128)} %copy-done.1, f32[12,24,8]{1,2,0:T(8,128)S(1)} %get-tuple-element.21, pred[12,384]{1,0:T(8,128)(4,1)S(1)} %broadcast_compare_fusion.1), kind=kOutput, calls=%fused_computation.12 | convolution fusion | flops 115900416 | bytes 8861184 | tf_op jit(solution)/shard_map/snhj,sjhd->snhd/dot_general | solution.py:88
  146.4 1.6 reshape.103
  148.0 6.0 %all-to-all-start.1 = ((f32[8,1,18432]{2,1,0:T(1,128)}), f32[8,1,18432]{2,1,0:T(1,128)S(1)}, u32[]{:S(2)}, u32[]{:S(2)}) async-start(f32[8,1,18432]{2,1,0:T(1,128)} %reshape.103), calls=%async_computation.1 | async-start | bytes 1179648 | tf_op jit(solution)/shard_map/all_to_all | solution.py:112
  154.2 1.6 fusion.54
  155.9 1.3 reshape_squeeze.11
  157.2 1.3 convolution_bitcast_fusion
  158.5 1.2 copy.74
  162.9 6.0 %all-to-all-done.1 = f32[8,1,18432]{2,1,0:T(1,128)S(1)} async-done(((f32[8,1,18432]{2,1,0:T(1,128)}), f32[8,1,18432]{2,1,0:T(1,128)S(1)}, u32[]{:S(2)}, u32[]{:S(2)}) %all-to-all-start.1) | async-done | bytes 589856 | tf_op jit(solution)/shard_map/all_to_all | solution.py:112
  168.9 2.0 reduce
  172.9 31.0 %all-gather = bf16[8,36,512]{2,1,0:T(8,128)(2,1)S(1)} all-gather(bf16[1,36,512]{2,1,0:T(8,128)(2,1)S(1)} %reshape.100), channel_id=1, replica_groups=mesh['kv'=8,'tp'=4] {'kv'}, dimensions={0}, use_global_device_ids=true | all-gather | bytes 331776 | tf_op jit(solution)/shard_map/all_gather | solution.py:127
  205.1 19.4 %reduce-scatter.2.cloned.1.call-done = bf16[72,512]{1,0:T(8,128)(2,1)} async-done(((bf16[288,512]{1,0:T(8,128)(2,1)}), bf16[72,512]{1,0:T(8,128)(2,1)}) %reduce-scatter.2.cloned.1.call-update) | async-done | bytes 73744 | tf_op jit(solution)/shard_map/reduce_scatter | solution.py:129
  (85 shorter events, 18.9 us)
Async XLA Ops:
  6.5 1.2 copy-start
  6.5 3.8 %copy-start.2 = (bf16[288,512]{1,0:T(8,128)(2,1)S(1)}, bf16[288,512]{1,0:T(8,128)(2,1)}, u32[]{:S(2)}) copy-start(bf16[288,512]{1,0:T(8,128)(2,1)} %param.13) | copy-start | bytes 884740
  6.5 3.8 %copy-start.9 = (f32[512]{0:T(512)S(1)}, f32[512]{0:T(512)}, u32[]{:S(2)}) copy-start(f32[512]{0:T(512)} %param.14) | copy-start | bytes 6148
  6.5 2.5 %copy-start.3 = (bf16[512,512]{1,0:T(8,128)(2,1)S(1)}, bf16[512,512]{1,0:T(8,128)(2,1)}, u32[]{:S(2)}) copy-start(bf16[512,512]{1,0:T(8,128)(2,1)} %param.16) | copy-start | bytes 1572868
  6.5 3.8 %copy-start.4 = (bf16[512,512]{1,0:T(8,128)(2,1)S(1)}, bf16[512,512]{1,0:T(8,128)(2,1)}, u32[]{:S(2)}) copy-start(bf16[512,512]{1,0:T(8,128)(2,1)} %param.17) | copy-start | bytes 1572868
  6.5 103.0 %all-reduce.3.cloned.1.call-start = ((), (), s32[]{:S(2)}) async-start(), calls=%async_computation.4 | async-start | bytes 3538944 | tf_op jit(solution)/shard_map/psum | solution.py:64
  12.1 42.2 %copy-start.11 = (f32[32]{0:T(128)S(1)}, f32[32]{0:T(128)}, u32[]{:S(2)}) copy-start(f32[32]{0:T(128)} %param.19) | copy-start | bytes 388
  54.5 6.7 %copy-start.12 = (s32[12]{0:T(128)S(1)}, s32[12]{0:T(128)}, u32[]{:S(2)}) copy-start(s32[12]{0:T(128)} %param.24) | copy-start | bytes 148
  54.5 6.7 %copy-start.10 = (s32[12,24]{1,0:T(8,128)S(1)}, s32[12,24]{1,0:T(8,128)}, u32[]{:S(2)}) copy-start(s32[12,24]{1,0:T(8,128)} %param.25) | copy-start | bytes 3460
  63.6 48.7 %copy-start.7 = (f32[12,24,8]{1,2,0:T(8,128)}, f32[12,24,8]{1,2,0:T(8,128)S(1)}, u32[]{:S(2)}) copy-start(f32[12,24,8]{1,2,0:T(8,128)S(1)} %fusion.37) | copy-start | bytes 27652
  111.2 1.2 copy-start.8
  115.5 1.8 copy-start.1
  120.7 13.1 %all-to-all-start.2 = ((f32[8,1,288]{2,1,0:T(1,128)}), f32[8,1,288]{2,1,0:T(1,128)S(1)}, u32[]{:S(2)}, u32[]{:S(2)}) async-start(f32[8,1,288]{2,1,0:T(1,128)} %reshape.107), calls=%async_computation.2 | async-start | bytes 24576 | tf_op jit(solution)/shard_map/all_to_all | solution.py:111
  133.8 14.2 %all-to-all-start = ((f32[8,1,288]{2,1,0:T(1,128)}), f32[8,1,288]{2,1,0:T(1,128)S(1)}, u32[]{:S(2)}, u32[]{:S(2)}) async-start(f32[8,1,288]{2,1,0:T(1,128)} %reshape.105), calls=%async_computation | async-start | bytes 24576 | tf_op jit(solution)/shard_map/all_to_all | solution.py:110
  148.0 20.9 %all-to-all-start.1 = ((f32[8,1,18432]{2,1,0:T(1,128)}), f32[8,1,18432]{2,1,0:T(1,128)S(1)}, u32[]{:S(2)}, u32[]{:S(2)}) async-start(f32[8,1,18432]{2,1,0:T(1,128)} %reshape.103), calls=%async_computation.1 | async-start | bytes 1179648 | tf_op jit(solution)/shard_map/all_to_all | solution.py:112
  154.0 70.5 %reduce-scatter.2.cloned.1.call-start = ((), (), s32[]{:S(2)}) async-start(), calls=%async_computation.5 | async-start | bytes 368640 | tf_op jit(solution)/shard_map/reduce_scatter | solution.py:129
  158.5 1.3 copy-start.6
  171.3 32.7 %copy-start.5 = (bf16[512,512]{1,0:T(8,128)(2,1)S(1)}, bf16[512,512]{1,0:T(8,128)(2,1)}, u32[]{:S(2)}) copy-start(bf16[512,512]{1,0:T(8,128)(2,1)} %param.20) | copy-start | bytes 1572868
Sparse Core Ops, SparseCore 0:
  12.2 97.2 all-reduce.2
  205.2 19.2 reduce-scatter.1
where the time goes:
time: 232 us; the launch traced here: 231 us
  blocking collectives  72 us (31%)
  waiting for transfers between devices  71.4 us (31%)
  local copies, waits for them, and re-layouts  27.7 us (12%)
  matrix products  18.5 us (8%)
  starting transfers between devices  16.3 us (7%)
  between operations  13.8 us (6%)
  other arithmetic  11.5 us (5%)
    psum x1, waiting for transfers between devices, body(): stacked, gate_part, squares = lax.psum((stacked, gate_part, squares), 'kv')  45.9 us
    psum x1, blocking collectives, body(): stacked, gate_part, squares = lax.psum((stacked, gate_part, squares), 'kv')  41 us
    all_gather x1, blocking collectives, body(): lax.all_gather(piece.reshape(block, heads_dev * head_dim), 'kv', axis=0,...  31 us
    unnamed x36, local copies, waits for them, and re-layouts  20.3 us
    reduce_scatter x1, waiting for transfers between devices, body(): lax.psum_scatter(term.astype(jnp.bfloat16), 'tp', scatter_dimension=0, ti...  19.4 us
    all_to_all x1, waiting for transfers between devices, body(): lax.all_to_all(cache_mix[None], 'kv', split_axis=1, concat_axis=0, tiled=...  6.02 us
    all_to_all x1, starting transfers between devices, body(): lax.all_to_all(cache_top[None], 'kv', split_axis=1, concat_axis=0, tiled=...  6 us
    all_to_all x1, starting transfers between devices, body(): lax.all_to_all(cache_mix[None], 'kv', split_axis=1, concat_axis=0, tiled=...  6 us
  transfers between devices with their start and end apart: 5, of which 3 were waited for; matrix products, arithmetic and copies ran while one was open for 16% of the time, Pallas kernels for 0%

commit v1 on v0

v1 whole, which is shorter than its diff:
```python
import functools

import jax
import jax.numpy as jnp
from jax import lax
from jax.experimental import pallas as pl
from jax.experimental.pallas import tpu as pltpu
from jax.sharding import PartitionSpec as P

F32 = jnp.float32
BF16 = jnp.bfloat16
LANES = 128
LOW = -1e30
NT = (((1,), (1,)), ((), ()))
HIGH = lax.Precision.HIGHEST


def dot(a, b, precision=None):
    return jnp.dot(a, b, preferred_element_type=F32, precision=precision)


def dot_nt(a, b, precision=None):
    return lax.dot_general(a, b, NT, preferred_element_type=F32, precision=precision)


def fold(x):
    half = x.shape[1] // 2
    return jnp.concatenate([x[:, :half], x[:, half:]], axis=0)


def unfold(x):
    rows = x.shape[0] // 2
    x = x.astype(F32)
    return jnp.concatenate([x[:rows], x[rows:]], axis=1)


def kernel(
    n,
    n_tp,
    tokens,
    gain,
    query_w,
    key_w,
    value_w,
    gate_hbm,
    bias,
    out_hbm,
    keys_hbm,
    values_hbm,
    decay,
    lengths,
    parents,
    out,
    part,
    part_in,
    gate_w,
    out_w,
    keys,
    values,
    qbuf,
    mix,
    stat,
    mix_in,
    stat_in,
    att,
    anc,
    path_s,
    tmix,
    tstat,
    kvnew,
    terms,
    terms_in,
    par_pad,
    load_sem,
    cache_sem,
    a_send,
    a_recv,
    b_send,
    b_recv,
    c_send,
    c_recv,
    d_send,
    d_recv,
    e_send,
    e_recv,
):
    me = lax.axis_index("kv")
    tp = lax.axis_index("tp")
    rows, depth = tokens.shape
    seqs, props = parents.shape
    heads = decay.shape[1]
    pos_dev = keys.shape[1]
    width = query_w.shape[1]
    head_dim = width // heads
    scale = head_dim ** (-0.5)
    slots = part_in.shape[1]
    parity = lax.rem(tp, 2)
    left_over = seqs % n
    hp = heads * props

    barrier = pltpu.get_barrier_semaphore()
    for k in range(1, n):
        pl.semaphore_signal(barrier, inc=1, device_id={"kv": lax.rem(me + k, n)})
    for k in range(1, n_tp):
        pl.semaphore_signal(barrier, inc=1, device_id={"tp": lax.rem(tp + k, n_tp)})

    gate_load = pltpu.make_async_copy(
        gate_hbm.at[pl.ds(pl.multiple_of(me * depth, depth), depth), :], gate_w, load_sem.at[0]
    )
    gate_load.start()
    cache_loads = []
    for s in range(seqs):
        k_load = pltpu.make_async_copy(keys_hbm.at[s], keys.at[s], cache_sem.at[0, s])
        v_load = pltpu.make_async_copy(values_hbm.at[s], values.at[s], cache_sem.at[1, s])
        k_load.start()
        v_load.start()
        cache_loads.append((k_load, v_load))
    out_load = pltpu.make_async_copy(out_hbm, out_w, load_sem.at[1])
    out_load.start()

    def owner_of(s):
        if isinstance(s, int):
            place = s % n
            shift = parity * left_over if s // n == seqs // n else 0
        else:
            place = lax.rem(s, n)
            shift = jnp.where(lax.div(s, n) == seqs // n, parity * left_over, 0)
        return lax.rem(place + shift, n)

    def slot_seq(r):
        shift = parity * left_over if r == seqs // n else 0
        return r * n + lax.rem(me + 2 * n - shift, n)

    def for_slot(r, f):
        if (r + 1) * n <= seqs:
            f()
        else:
            pl.when(slot_seq(r) < seqs)(f)

    xf = tokens[...].astype(F32)
    squares = jnp.sum(xf * xf, axis=1, keepdims=True)
    normed = (xf * gain[...]).astype(BF16)
    sel_rows = lax.broadcasted_iota(jnp.int32, (bias.shape[1], LANES), 0)
    sel_cols = lax.broadcasted_iota(jnp.int32, (bias.shape[1], LANES), 1)
    select = ((sel_rows == sel_cols + tp * heads) & (sel_cols < heads)).astype(F32)
    for i, w in enumerate((query_w, key_w, value_w)):
        part[:, :, i * width : (i + 1) * width] = dot(normed, w[...]).reshape(seqs, props, width)
    gate_load.wait()
    gates_w = dot(gate_w[...], select.astype(BF16)).astype(BF16)
    gate_part = dot(normed, gates_w)
    lane = lax.broadcasted_iota(jnp.int32, (rows, LANES), 1)
    gate_part = jnp.where(lane == LANES // 2, squares, gate_part)
    part[:, :, 3 * width :] = gate_part.reshape(seqs, props, LANES)
    pl.semaphore_wait(barrier, n + n_tp - 2)

    def a_copy(s):
        d = owner_of(s)
        k = lax.rem(me - d + n, n)
        return d, pltpu.make_async_remote_copy(
            src_ref=part.at[s],
            dst_ref=part_in.at[jnp.maximum(k - 1, 0), s // n],
            send_sem=a_send.at[s],
            recv_sem=a_recv.at[jnp.maximum(k - 1, 0), s // n],
            device_id={"kv": d},
        )

    for s in range(seqs):
        d, copy = a_copy(s)
        pl.when(d != me)(copy.start)

    par_pad[...] = jnp.zeros(par_pad.shape, jnp.int32)
    par_pad[0:seqs, 0:props] = parents[...]
    r_i = lax.broadcasted_iota(jnp.int32, (LANES, LANES), 0)
    c_i = lax.broadcasted_iota(jnp.int32, (LANES, LANES), 1)
    eye = (r_i == c_i).astype(F32)
    bias_row = dot(jnp.broadcast_to(bias[...], (8, bias.shape[1])), select, HIGH)[0:1]

    def ancestry(r):
        s = slot_seq(r)
        row = par_pad[pl.ds(s, 1), :]
        link = jnp.maximum((row == r_i).astype(F32), eye).astype(BF16)
        for _ in range(props.bit_length()):
            link = jnp.minimum(dot(link, link), 1.0).astype(BF16)
        anc[r] = dot_nt(eye.astype(BF16), link)[:props]

    for r in range(slots):
        for_slot(r, functools.partial(ancestry, r))

    lane_p = lax.broadcasted_iota(jnp.int32, (props, LANES), 1)
    bd_row = lax.broadcasted_iota(jnp.int32, (heads, props, width), 0)
    bd_col = lax.broadcasted_iota(jnp.int32, (heads, props, width), 2)
    diag = (lax.div(bd_col, head_dim) == bd_row).reshape(hp, width)

    def spread(q):
        wide = jnp.broadcast_to(q[None], (heads, props, width)).reshape(hp, width)
        return jnp.where(diag, wide, 0.0).astype(BF16)

    def gather_diag(m):
        return jnp.sum(jnp.where(diag, m, 0.0).reshape(heads, props, width), axis=0)

    def to_lanes(col, first):
        acc = jnp.zeros((props, LANES), F32)
        for h in range(heads):
            acc = jnp.where(lane_p == h + first, col[h * props : (h + 1) * props], acc)
        return acc

    def b_copy(r, k, buf, send, recv):
        s = slot_seq(r)
        return pltpu.make_async_remote_copy(
            src_ref=buf.at[s],
            dst_ref=buf.at[s],
            send_sem=send.at[r, k - 1],
            recv_sem=recv.at[s],
            device_id={"kv": lax.rem(me + k, n)},
        )

    pad_rows = LANES - props

    def project(r):
        s = slot_seq(r)
        for k in range(1, n):
            pltpu.make_async_remote_copy(
                src_ref=part.at[0],
                dst_ref=part_in.at[k - 1, r],
                send_sem=a_send.at[0],
                recv_sem=a_recv.at[k - 1, r],
                device_id={"kv": lax.rem(me + k, n)},
            ).wait_recv()
        total = part[s]
        for k in range(1, n):
            total = total + part_in[k - 1, r]
        tail = total[:, 3 * width :]
        square = jnp.sum(jnp.where(lane_p == LANES // 2, tail, 0.0), axis=1, keepdims=True)
        inverse = lax.rsqrt(square / (depth * n) + 1e-06)
        q = inverse * total[:, :width]
        qbuf[s] = fold(q).astype(BF16)
        for k in range(1, n):
            b_copy(r, k, qbuf, b_send, b_recv).start()
        kvnew[r, 0, 0:props] = inverse * total[:, width : 2 * width]
        kvnew[r, 1, 0:props] = inverse * total[:, 2 * width : 3 * width]
        kvnew[r, :, props:] = jnp.zeros((2, pad_rows, width), F32)
        x = inverse * tail + bias_row
        log_gate = jnp.minimum(x, 0.0) - jnp.log1p(jnp.exp(-jnp.abs(x)))
        padded = jnp.concatenate([log_gate, jnp.zeros((pad_rows, LANES), F32)], axis=0)
        path_s[r] = dot(anc[r], padded, HIGH)

    for r in range(slots):
        for_slot(r, functools.partial(project, r))

    def tree(r):
        s = slot_seq(r)
        path = path_s[r]
        q = spread(unfold(qbuf[s]))
        head_of = lax.broadcasted_iota(jnp.int32, (heads, props, LANES), 0)
        lane_of = lax.broadcasted_iota(jnp.int32, (heads, props, LANES), 2)
        pick = (head_of == lane_of).reshape(hp, LANES)
        tiled = jnp.broadcast_to(path[None], (heads, props, LANES)).reshape(hp, LANES)
        own = jnp.sum(jnp.where(pick, tiled, 0.0), axis=1, keepdims=True)
        padded = jnp.concatenate([path, jnp.zeros((pad_rows, LANES), F32)], axis=0)
        other = dot_nt(pick.astype(F32), padded, HIGH)
        scores = dot_nt(q, kvnew[r, 0].astype(BF16)) * scale + own - other
        live = jnp.broadcast_to(anc[r][None], (heads, props, LANES)).reshape(hp, LANES) > 0.5
        scores = jnp.where(live, scores, LOW)
        top = jnp.max(scores, axis=1, keepdims=True)
        w = jnp.where(live, jnp.exp(scores - top), 0.0)
        total = jnp.sum(w, axis=1, keepdims=True)
        tmix[r] = gather_diag(dot(w.astype(BF16), kvnew[r, 1].astype(BF16)))
        tstat[r, 0] = to_lanes(top, 0)
        tstat[r, 1] = to_lanes(total, 0)

    for r in range(slots):
        for_slot(r, functools.partial(tree, r))

    position = lax.broadcasted_iota(jnp.int32, (hp, pos_dev), 1) + me * pos_dev

    def c_copy(s, which, src, dst):
        d = owner_of(s)
        k = jnp.maximum(lax.rem(me - d + n, n) - 1, 0)
        slot = s // n if isinstance(s, int) else lax.div(s, n)
        return d, pltpu.make_async_remote_copy(
            src_ref=src.at[s],
            dst_ref=dst.at[k, slot],
            send_sem=c_send.at[which, s],
            recv_sem=c_recv.at[which, k, slot],
            device_id={"kv": d},
        )

    def shard(s, carry):
        d = owner_of(s)

        @pl.when(d != me)
        def _():
            pltpu.make_async_remote_copy(
                src_ref=qbuf.at[s],
                dst_ref=qbuf.at[s],
                send_sem=b_send.at[0, 0],
                recv_sem=b_recv.at[s],
                device_id={"kv": d},
            ).wait_recv()

        pltpu.make_async_copy(keys_hbm.at[s], keys.at[s], cache_sem.at[0, s]).wait()
        pltpu.make_async_copy(values_hbm.at[s], values.at[s], cache_sem.at[1, s]).wait()
        q = spread(unfold(qbuf[s]))
        fade = decay[s]
        fade = jnp.concatenate(
            [jnp.broadcast_to(fade[h : h + 1], (props, pos_dev)) for h in range(heads)], axis=0
        )
        scores = dot_nt(q, keys[s]) * scale + fade
        live = position < lengths[s]
        scores = jnp.where(live, scores, LOW)
        top = jnp.max(scores, axis=1, keepdims=True)
        w = jnp.where(live, jnp.exp(scores - top), 0.0)
        total = jnp.sum(w, axis=1, keepdims=True)
        mix[s] = fold(gather_diag(dot(w.astype(BF16), values[s]))).astype(BF16)
        stat[s] = to_lanes(top, 0) + to_lanes(total, heads)
        for which, (src, dst) in enumerate(((mix, mix_in), (stat, stat_in))):
            _, copy = c_copy(s, which, src, dst)
            pl.when(d != me)(copy.start)
        return carry

    lax.fori_loop(0, seqs, shard, 0)

    ex_r = lax.broadcasted_iota(jnp.int32, (LANES, width), 0)
    ex_c = lax.broadcasted_iota(jnp.int32, (LANES, width), 1)
    widen = (ex_r == lax.div(ex_c, head_dim)).astype(F32)

    def merge(r):
        s = slot_seq(r)
        for k in range(1, n):
            for which, (src, dst) in enumerate(((mix, mix_in), (stat, stat_in))):
                pltpu.make_async_remote_copy(
                    src_ref=src.at[0],
                    dst_ref=dst.at[k - 1, r],
                    send_sem=c_send.at[which, 0],
                    recv_sem=c_recv.at[which, k - 1, r],
                    device_id={"kv": lax.rem(me + k, n)},
                ).wait_recv()
        stats = jnp.concatenate([stat[s]] + [stat_in[k, r] for k in range(n - 1)], axis=0)
        totals = pltpu.roll(stats, LANES - heads, 1).reshape(n, props, LANES)
        tops = stats.reshape(n, props, LANES) + path_s[r][None]
        tops = jnp.where((lane_p < heads)[None], tops, LOW)
        ttop = jnp.where(lane_p < heads, tstat[r, 0], LOW)
        best = jnp.maximum(jnp.max(tops, axis=0), ttop)
        factors = jnp.exp(tops - best[None])
        tfactor = jnp.exp(ttop - best)
        denom = jnp.sum(factors * totals, axis=0) + tfactor * tstat[r, 1]
        packed = jnp.concatenate([factors.reshape(n * props, LANES), tfactor, denom], axis=0)
        wide = dot(packed, widen, HIGH)
        numer = wide[n * props : (n + 1) * props] * tmix[r] + wide[:props] * unfold(mix[s])
        for k in range(1, n):
            numer = numer + wide[k * props : (k + 1) * props] * unfold(mix_in[k - 1, r])
        att[s] = fold(numer / wide[(n + 1) * props :]).astype(BF16)
        for k in range(1, n):
            b_copy(r, k, att, d_send, d_recv).start()

    for r in range(slots):
        for_slot(r, functools.partial(merge, r))

    for s in range(seqs):
        d = owner_of(s)

        @pl.when(d != me)
        def _(s=s, d=d):
            pltpu.make_async_remote_copy(
                src_ref=att.at[s],
                dst_ref=att.at[s],
                send_sem=d_send.at[0, 0],
                recv_sem=d_recv.at[s],
                device_id={"kv": d},
            ).wait_recv()

    out_load.wait()
    attended = jnp.concatenate([unfold(att[s]) for s in range(seqs)], axis=0).astype(BF16)
    block = rows // n_tp
    term = dot(attended, out_w[...])
    for t in range(n_tp):
        terms[t] = term[t * block : (t + 1) * block].astype(BF16)

    def e_copy(k):
        t = lax.rem(tp + k, n_tp)
        return pltpu.make_async_remote_copy(
            src_ref=terms.at[t],
            dst_ref=terms_in.at[n_tp - k - 1],
            send_sem=e_send.at[k - 1],
            recv_sem=e_recv.at[n_tp - k - 1],
            device_id={"tp": t},
        )

    for k in range(1, n_tp):
        e_copy(k).start()
    total = terms[tp].astype(F32)
    for k in range(1, n_tp):
        e_copy(n_tp - k).wait_recv()
        total = total + terms_in[k - 1].astype(F32)
    out[...] = total.astype(BF16)

    for s in range(seqs):
        d, copy = a_copy(s)
        pl.when(d != me)(copy.wait_send)
        for which, (src, dst) in enumerate(((mix, mix_in), (stat, stat_in))):
            _, copy = c_copy(s, which, src, dst)
            pl.when(d != me)(copy.wait_send)
    for r in range(slots):

        def drain(r=r):
            for k in range(1, n):
                b_copy(r, k, qbuf, b_send, b_recv).wait_send()
                b_copy(r, k, att, d_send, d_recv).wait_send()

        for_slot(r, drain)
    for k in range(1, n_tp):
        e_copy(k).wait_send()


def solution(mesh):
    n, n_tp = mesh.shape["kv"], mesh.shape["tp"]

    def body(
        tokens,
        norm_gain,
        query_weight,
        key_weight,
        value_weight,
        gate_weight,
        gate_bias,
        out_weight,
        cache_keys,
        cache_values,
        cache_decay,
        lengths,
        parents,
    ):
        rows, depth = tokens.shape
        seqs, props = parents.shape
        heads = cache_decay.shape[1]
        pos_dev = cache_keys.shape[1]
        width = query_weight.shape[1]
        cols = out_weight.shape[1]
        slots = -(-seqs // n)
        block = rows // n_tp
        all_w = 3 * width + LANES
        folded = (2 * props, width // 2)
        vmem = pl.BlockSpec(memory_space=pltpu.VMEM)
        hbm = pl.BlockSpec(memory_space=pl.ANY)
        smem = pl.BlockSpec(memory_space=pltpu.SMEM)
        dma = pltpu.SemaphoreType.DMA
        return pl.pallas_call(
            functools.partial(kernel, n, n_tp),
            out_shape=jax.ShapeDtypeStruct((block, cols), BF16),
            in_specs=[vmem, vmem, vmem, vmem, vmem, hbm, vmem, hbm, hbm, hbm, vmem, smem, vmem],
            out_specs=vmem,
            scratch_shapes=[
                pltpu.VMEM((seqs, props, all_w), F32),
                pltpu.VMEM((n - 1, slots, props, all_w), F32),
                pltpu.VMEM((depth, gate_weight.shape[1]), BF16),
                pltpu.VMEM(out_weight.shape, BF16),
                pltpu.VMEM(cache_keys.shape, BF16),
                pltpu.VMEM(cache_values.shape, BF16),
                pltpu.VMEM((seqs,) + folded, BF16),
                pltpu.VMEM((seqs,) + folded, BF16),
                pltpu.VMEM((seqs, props, LANES), F32),
                pltpu.VMEM((n - 1, slots) + folded, BF16),
                pltpu.VMEM((n - 1, slots, props, LANES), F32),
                pltpu.VMEM((seqs,) + folded, BF16),
                pltpu.VMEM((slots, props, LANES), F32),
                pltpu.VMEM((slots, props, LANES), F32),
                pltpu.VMEM((slots, props, width), F32),
                pltpu.VMEM((slots, 2, props, LANES), F32),
                pltpu.VMEM((slots, 2, LANES, width), F32),
                pltpu.VMEM((n_tp, block, cols), BF16),
                pltpu.VMEM((n_tp - 1, block, cols), BF16),
                pltpu.VMEM((-(-seqs // 8) * 8, LANES), jnp.int32),
                dma((2,)),
                dma((2, seqs)),
                dma((seqs,)),
                dma((n - 1, slots)),
                dma((slots, n - 1)),
                dma((seqs,)),
                dma((2, seqs)),
                dma((2, n - 1, slots)),
                dma((slots, n - 1)),
                dma((seqs,)),
                dma((n_tp - 1,)),
                dma((n_tp - 1,)),
            ],
            compiler_params=pltpu.CompilerParams(
                collective_id=0, has_side_effects=True, vmem_limit_bytes=48 * 1024 * 1024
            ),
        )(
            tokens,
            norm_gain.reshape(1, depth),
            query_weight,
            key_weight,
            value_weight,
            gate_weight,
            gate_bias.reshape(1, gate_bias.shape[0]),
            out_weight,
            cache_keys,
            cache_values,
            cache_decay,
            lengths,
            parents,
        )

    in_specs = (
        P(None, "kv"),
        P("kv"),
        P("kv", "tp"),
        P("kv", "tp"),
        P("kv", "tp"),
        P(),
        P(),
        P("tp", "kv"),
        P(None, "kv", "tp"),
        P(None, "kv", "tp"),
        P(None, "tp", "kv"),
        P(),
        P(),
    )
    out_specs = P("tp", "kv")
    return jax.shard_map(body, mesh=mesh, in_specs=in_specs, out_specs=out_specs, check_vma=False)
```

time: 232 us -> 91.8 us (0.40)
  Pallas kernels: 0 us -> 80.4 us
  blocking collectives: 72 us -> 0 us
  waiting for transfers between devices: 71.4 us -> 0 us
  matrix products: 18.5 us -> 0 us
  local copies, waits for them, and re-layouts: 27.7 us -> 10.8 us
  starting transfers between devices: 16.3 us -> 0 us
  between operations: 13.8 us -> 0.03 us
  other arithmetic: 11.5 us -> 0 us
    pallas_call x0 -> x1, Pallas kernels: none -> 80.4 us  [body(): pl.pallas_call(functools.partial(kernel, n, n_tp), out_shape=jax.ShapeDty...]
    psum x1 -> x0, waiting for transfers between devices: 45.9 us -> none  [body(): stacked, gate_part, squares = lax.psum((stacked, gate_part, squares), 'kv')]
    psum x1 -> x0, blocking collectives: 41 us -> none  [body(): stacked, gate_part, squares = lax.psum((stacked, gate_part, squares), 'kv')]
    all_gather x1 -> x0, blocking collectives: 31 us -> none  [body(): lax.all_gather(piece.reshape(block, heads_dev * head_dim), 'kv', axis=0,...]
    reduce_scatter x1 -> x0, waiting for transfers between devices: 19.4 us -> none  [body(): lax.psum_scatter(term.astype(jnp.bfloat16), 'tp', scatter_dimension=0, ti...]
    dot_general x15 -> x0, matrix products: 18.5 us -> none  [the longest x1 5.22 us: body(): jnp.einsum('snhj,sjhd->snhd', weights.astype(jnp.bfloat16), values, prefe...]
    all_to_all x3 -> x0, starting transfers between devices: 16 us -> none  [the longest x1 6 us: body(): lax.all_to_all(cache_top[None], 'kv', split_axis=1, concat_axis=0, tiled=...]
    unnamed x36 -> x22, local copies, waits for them, and re-layouts: 20.3 us -> 10.8 us
  transfers between devices with their start and end apart: 5 -> 0, of which waited for: 3 -> 0; matrix products, arithmetic and copies ran while one was open for 16% -> 0% of each run, Pallas kernels for 0% -> 0%
where the time goes in v1:
time: 91.8 us; the launch traced here: 91.2 us
  Pallas kernels  80.4 us (88%)
  local copies, waits for them, and re-layouts  10.8 us (12%)
    pallas_call x1, Pallas kernels, body(): pl.pallas_call(functools.partial(kernel, n, n_tp), out_shape=jax.ShapeDty...  80.4 us
    unnamed x22, local copies, waits for them, and re-layouts  10.8 us

profile of v1, /device:TPU:0, one launch (start us, length us, event | category | flops | bytes accessed | tf_op | source)
XLA Modules:
  0.0 91.2 jit_solution(14293169362628424778)
XLA Ops:
  0.0 1.4 %copy.14.gate_hbm = bf16[4096,32]{1,0:T(8,128)(2,1)S(1)} copy(bf16[4096,32]{0,1:T(8,128)(2,1)} %param.18) | data formatting | bytes 524288 | tf_op args[5]
  1.4 0.0 copy-start
  1.4 1.0 %copy-done = bf16[512,512]{1,0:T(8,128)(2,1)S(1)} copy-done((bf16[512,512]{1,0:T(8,128)(2,1)S(1)}, bf16[512,512]{1,0:T(8,128)(2,1)}, u32[]{:S(2)}) %copy-start) | copy-done | bytes 524312
  2.5 0.0 copy-start.1
  2.5 1.0 %copy-done.1 = bf16[512,512]{1,0:T(8,128)(2,1)S(1)} copy-done((bf16[512,512]{1,0:T(8,128)(2,1)S(1)}, bf16[512,512]{1,0:T(8,128)(2,1)}, u32[]{:S(2)}) %copy-start.1) | copy-done | bytes 524312
  3.5 0.0 copy-start.2
  3.5 1.0 %copy-done.2 = bf16[512,512]{1,0:T(8,128)(2,1)S(1)} copy-done((bf16[512,512]{1,0:T(8,128)(2,1)S(1)}, bf16[512,512]{1,0:T(8,128)(2,1)}, u32[]{:S(2)}) %copy-start.2) | copy-done | bytes 524312
  4.6 0.0 copy-start.3
  4.6 1.0 %copy-done.3 = bf16[512,512]{1,0:T(8,128)(2,1)S(1)} copy-done((bf16[512,512]{1,0:T(8,128)(2,1)S(1)}, bf16[512,512]{1,0:T(8,128)(2,1)}, u32[]{:S(2)}) %copy-start.3) | copy-done | bytes 524312
  5.6 0.0 copy-start.4
  5.6 1.0 %copy-done.4 = bf16[288,512]{1,0:T(8,128)(2,1)S(1)} copy-done((bf16[288,512]{1,0:T(8,128)(2,1)S(1)}, bf16[288,512]{1,0:T(8,128)(2,1)}, u32[]{:S(2)}) %copy-start.4) | copy-done | bytes 294936
  6.6 0.0 copy-start.5
  6.6 0.9 copy-done.5
  7.5 0.0 copy-start.6
  7.5 0.7 copy-done.6
  8.2 0.0 copy-start.7
  8.2 0.7 copy-done.7
  8.9 0.0 copy-start.8
  8.9 0.7 copy-done.8
  9.5 0.0 copy-start.9
  9.5 0.7 copy-done.9
  10.2 80.4 %shard_map.127 = bf16[72,512]{1,0:T(8,128)(2,1)S(1)} custom-call(bf16[288,512]{1,0:T(8,128)(2,1)S(1)} %copy-done.4, f32[1,512]{1,0:T(1,128)S(1)} %bitcast.2, bf16[512,512]{1,0:T(8,128)(2,1)S(1)} %copy-done, bf16[512,512]{1,0:T(8,128)(2,1)S(1)} %copy-done.1, bf16[512,512]{1,0:T(8,128)(2,1)S(1)} %copy-done.2, bf16[4096,32]{1,0:T(8,128)(2,1)S(1)} %copy.14.gate_hbm, ...), custom_call_target="tpu_custom_call" | custom-call | tf_op jit(solution)/shard_map/pallas_call | solution.py:447
  90.6 0.6 copy.16
Async XLA Ops:
  1.4 1.0 %copy-start = (bf16[512,512]{1,0:T(8,128)(2,1)S(1)}, bf16[512,512]{1,0:T(8,128)(2,1)}, u32[]{:S(2)}) copy-start(bf16[512,512]{1,0:T(8,128)(2,1)} %query_w.1) | copy-start | bytes 1572868
  2.5 1.0 %copy-start.1 = (bf16[512,512]{1,0:T(8,128)(2,1)S(1)}, bf16[512,512]{1,0:T(8,128)(2,1)}, u32[]{:S(2)}) copy-start(bf16[512,512]{1,0:T(8,128)(2,1)} %key_w.1) | copy-start | bytes 1572868
  3.5 1.0 %copy-start.2 = (bf16[512,512]{1,0:T(8,128)(2,1)S(1)}, bf16[512,512]{1,0:T(8,128)(2,1)}, u32[]{:S(2)}) copy-start(bf16[512,512]{1,0:T(8,128)(2,1)} %value_w.1) | copy-start | bytes 1572868
  4.6 1.0 %copy-start.3 = (bf16[512,512]{1,0:T(8,128)(2,1)S(1)}, bf16[512,512]{1,0:T(8,128)(2,1)}, u32[]{:S(2)}) copy-start(bf16[512,512]{1,0:T(8,128)(2,1)} %out_hbm.1) | copy-start | bytes 1572868
  5.6 1.0 %copy-start.4 = (bf16[288,512]{1,0:T(8,128)(2,1)S(1)}, bf16[288,512]{1,0:T(8,128)(2,1)}, u32[]{:S(2)}) copy-start(bf16[288,512]{1,0:T(8,128)(2,1)} %tokens.1) | copy-start | bytes 884740
  6.6 0.9 copy-start.5
  7.5 0.7 copy-start.6
  8.2 0.7 copy-start.7
  8.9 0.7 copy-start.8
  9.5 0.7 copy-start.9

commit v2 on v1

--- a/solution.py
+++ b/solution.py
@@ -52,7 +52,11 @@
     parents,
     out,
     part,
+    part_v,
+    pair_in,
+    pair_in_v,
     part_in,
+    part_in_v,
     gate_w,
     out_w,
     keys,
@@ -73,6 +77,8 @@
     par_pad,
     load_sem,
     cache_sem,
+    p_send,
+    p_recv,
     a_send,
     a_recv,
     b_send,
@@ -143,30 +149,56 @@
     sel_rows = lax.broadcasted_iota(jnp.int32, (bias.shape[1], LANES), 0)
     sel_cols = lax.broadcasted_iota(jnp.int32, (bias.shape[1], LANES), 1)
     select = ((sel_rows == sel_cols + tp * heads) & (sel_cols < heads)).astype(F32)
-    for i, w in enumerate((query_w, key_w, value_w)):
+    for i, w in enumerate((query_w, key_w)):
         part[:, :, i * width : (i + 1) * width] = dot(normed, w[...]).reshape(seqs, props, width)
+    value_part = dot(normed, value_w[...])
+    for s in range(seqs):
+        part_v[s] = fold(value_part[s * props : (s + 1) * props]).astype(BF16)
     gate_load.wait()
     gates_w = dot(gate_w[...], select.astype(BF16)).astype(BF16)
     gate_part = dot(normed, gates_w)
     lane = lax.broadcasted_iota(jnp.int32, (rows, LANES), 1)
     gate_part = jnp.where(lane == LANES // 2, squares, gate_part)
-    part[:, :, 3 * width :] = gate_part.reshape(seqs, props, LANES)
+    part[:, :, 2 * width :] = gate_part.reshape(seqs, props, LANES)
     pl.semaphore_wait(barrier, n + n_tp - 2)
 
-    def a_copy(s):
+    side = lax.rem(me, 2)
+    partner = me + 1 - 2 * side
+    n_far = n // 2
+    shares = ((part, pair_in, part_in), (part_v, pair_in_v, part_in_v))
+
+    def p_copy(s, which):
+        src, dst, _ = shares[which]
+        return pltpu.make_async_remote_copy(
+            src_ref=src.at[s],
+            dst_ref=dst.at[s],
+            send_sem=p_send.at[which, s],
+            recv_sem=p_recv.at[which, s],
+            device_id={"kv": partner},
+        )
+
+    def a_copy(s, which):
+        src, _, dst = shares[which]
         d = owner_of(s)
-        k = lax.rem(me - d + n, n)
-        return d, pltpu.make_async_remote_copy(
-            src_ref=part.at[s],
-            dst_ref=part_in.at[jnp.maximum(k - 1, 0), s // n],
-            send_sem=a_send.at[s],
-            recv_sem=a_recv.at[jnp.maximum(k - 1, 0), s // n],
+        k = jnp.maximum(lax.rem(lax.div(me, 2) - lax.div(d, 2) + n_far, n_far) - 1, 0)
+        return pltpu.make_async_remote_copy(
+            src_ref=src.at[s],
+            dst_ref=dst.at[k, s // n],
+            send_sem=a_send.at[which, s],
+            recv_sem=a_recv.at[which, k, s // n],
             device_id={"kv": d},
         )
 
+    def crosses(s):
+        return lax.rem(owner_of(s), 2) != side
+
+    def passes(s):
+        d = owner_of(s)
+        return (lax.rem(d, 2) == side) & (d != me)
+
     for s in range(seqs):
-        d, copy = a_copy(s)
-        pl.when(d != me)(copy.start)
+        for which in range(2):
+            pl.when(crosses(s))(p_copy(s, which).start)
 
     par_pad[...] = jnp.zeros(par_pad.shape, jnp.int32)
     par_pad[0:seqs, 0:props] = parents[...]
@@ -185,6 +217,17 @@
 
     for r in range(slots):
         for_slot(r, functools.partial(ancestry, r))
+
+    def pass_on(s):
+        for which in range(2):
+            p_copy(s, which).wait_recv()
+        part[s] = part[s] + pair_in[s]
+        part_v[s] = (part_v[s].astype(F32) + pair_in_v[s].astype(F32)).astype(BF16)
+        for which in range(2):
+            a_copy(s, which).start()
+
+    for s in range(seqs):
+        pl.when(passes(s))(functools.partial(pass_on, s))
 
     lane_p = lax.broadcasted_iota(jnp.int32, (props, LANES), 1)
     bd_row = lax.broadcasted_iota(jnp.int32, (heads, props, width), 0)
@@ -218,18 +261,28 @@
 
     def project(r):
         s = slot_seq(r)
-        for k in range(1, n):
+        for which, (src, near, far) in enumerate(shares):
             pltpu.make_async_remote_copy(
-                src_ref=part.at[0],
-                dst_ref=part_in.at[k - 1, r],
-                send_sem=a_send.at[0],
-                recv_sem=a_recv.at[k - 1, r],
-                device_id={"kv": lax.rem(me + k, n)},
+                src_ref=src.at[0],
+                dst_ref=near.at[s],
+                send_sem=p_send.at[which, 0],
+                recv_sem=p_recv.at[which, s],
+                device_id={"kv": partner},
             ).wait_recv()
-        total = part[s]
-        for k in range(1, n):
+            for k in range(1, n_far):
+                pltpu.make_async_remote_copy(
+                    src_ref=src.at[0],
+                    dst_ref=far.at[k - 1, r],
+                    send_sem=a_send.at[which, 0],
+                    recv_sem=a_recv.at[which, k - 1, r],
+                    device_id={"kv": lax.rem(me + 2 * k, n)},
+                ).wait_recv()
+        total = part[s] + pair_in[s]
+        total_v = unfold(part_v[s]) + unfold(pair_in_v[s])
+        for k in range(1, n_far):
             total = total + part_in[k - 1, r]
-        tail = total[:, 3 * width :]
+            total_v = total_v + unfold(part_in_v[k - 1, r])
+        tail = total[:, 2 * width :]
         square = jnp.sum(jnp.where(lane_p == LANES // 2, tail, 0.0), axis=1, keepdims=True)
         inverse = lax.rsqrt(square / (depth * n) + 1e-06)
         q = inverse * total[:, :width]
@@ -237,15 +290,12 @@
         for k in range(1, n):
             b_copy(r, k, qbuf, b_send, b_recv).start()
         kvnew[r, 0, 0:props] = inverse * total[:, width : 2 * width]
-        kvnew[r, 1, 0:props] = inverse * total[:, 2 * width : 3 * width]
+        kvnew[r, 1, 0:props] = inverse * total_v
         kvnew[r, :, props:] = jnp.zeros((2, pad_rows, width), F32)
         x = inverse * tail + bias_row
         log_gate = jnp.minimum(x, 0.0) - jnp.log1p(jnp.exp(-jnp.abs(x)))
         padded = jnp.concatenate([log_gate, jnp.zeros((pad_rows, LANES), F32)], axis=0)
         path_s[r] = dot(anc[r], padded, HIGH)
-
-    for r in range(slots):
-        for_slot(r, functools.partial(project, r))
 
     def tree(r):
         s = slot_seq(r)
@@ -268,9 +318,6 @@
         tstat[r, 0] = to_lanes(top, 0)
         tstat[r, 1] = to_lanes(total, 0)
 
-    for r in range(slots):
-        for_slot(r, functools.partial(tree, r))
-
     position = lax.broadcasted_iota(jnp.int32, (hp, pos_dev), 1) + me * pos_dev
 
     def c_copy(s, which, src, dst):
@@ -317,8 +364,6 @@
             _, copy = c_copy(s, which, src, dst)
             pl.when(d != me)(copy.start)
         return carry
-
-    lax.fori_loop(0, seqs, shard, 0)
 
     ex_r = lax.broadcasted_iota(jnp.int32, (LANES, width), 0)
     ex_c = lax.broadcasted_iota(jnp.int32, (LANES, width), 1)
@@ -354,49 +399,65 @@
             b_copy(r, k, att, d_send, d_recv).start()
 
     for r in range(slots):
-        for_slot(r, functools.partial(merge, r))
+        for_slot(r, functools.partial(project, r))
+        if r > 0:
+            for_slot(r - 1, functools.partial(merge, r - 1))
+        for_slot(r, functools.partial(tree, r))
+        lax.fori_loop(r * n, min((r + 1) * n, seqs), shard, 0)
+    for_slot(slots - 1, functools.partial(merge, slots - 1))
+
+    out_load.wait()
+    block = rows // n_tp
+
+    def e_copy(t):
+        k = lax.rem(tp - t + n_tp, n_tp)
+        return pltpu.make_async_remote_copy(
+            src_ref=terms.at[t],
+            dst_ref=terms_in.at[jnp.maximum(k - 1, 0)],
+            send_sem=e_send.at[t],
+            recv_sem=e_recv.at[jnp.maximum(k - 1, 0)],
+            device_id={"tp": t},
+        )
+
+    arrived = 0
+    for t in range(n_tp):
+        first, last = t * block // props, ((t + 1) * block - 1) // props + 1
+        for s in range(arrived, last):
+            d = owner_of(s)
+
+            @pl.when(d != me)
+            def _(s=s, d=d):
+                pltpu.make_async_remote_copy(
+                    src_ref=att.at[s],
+                    dst_ref=att.at[s],
+                    send_sem=d_send.at[0, 0],
+                    recv_sem=d_recv.at[s],
+                    device_id={"kv": d},
+                ).wait_recv()
+
+        arrived = max(arrived, last)
+        attended = jnp.concatenate([unfold(att[s]) for s in range(first, last)], axis=0)
+        term = dot(attended.astype(BF16), out_w[...])
+        begin = t * block - first * props
+        terms[t] = term[begin : begin + block].astype(BF16)
+        pl.when(tp != t)(e_copy(t).start)
+    total = terms[tp].astype(F32)
+    for k in range(1, n_tp):
+        pltpu.make_async_remote_copy(
+            src_ref=terms.at[0],
+            dst_ref=terms_in.at[k - 1],
+            send_sem=e_send.at[0],
+            recv_sem=e_recv.at[k - 1],
+            device_id={"tp": lax.rem(tp + k, n_tp)},
+        ).wait_recv()
+        total = total + terms_in[k - 1].astype(F32)
+    out[...] = total.astype(BF16)
 
     for s in range(seqs):
         d = owner_of(s)
-
-        @pl.when(d != me)
-        def _(s=s, d=d):
-            pltpu.make_async_remote_copy(
-                src_ref=att.at[s],
-                dst_ref=att.at[s],
-                send_sem=d_send.at[0, 0],
-                recv_sem=d_recv.at[s],
-                device_id={"kv": d},
-            ).wait_recv()
-
-    out_load.wait()
-    attended = jnp.concatenate([unfold(att[s]) for s in range(seqs)], axis=0).astype(BF16)
-    block = rows // n_tp
-    term = dot(attended, out_w[...])
-    for t in range(n_tp):
-        terms[t] = term[t * block : (t + 1) * block].astype(BF16)
-
-    def e_copy(k):
-        t = lax.rem(tp + k, n_tp)
-        return pltpu.make_async_remote_copy(
-            src_ref=terms.at[t],
-            dst_ref=terms_in.at[n_tp - k - 1],
-            send_sem=e_send.at[k - 1],
-            recv_sem=e_recv.at[n_tp - k - 1],
-            device_id={"tp": t},
-        )
-
-    for k in range(1, n_tp):
-        e_copy(k).start()
-    total = terms[tp].astype(F32)
-    for k in range(1, n_tp):
-        e_copy(n_tp - k).wait_recv()
-        total = total + terms_in[k - 1].astype(F32)
-    out[...] = total.astype(BF16)
-
-    for s in range(seqs):
-        d, copy = a_copy(s)
-        pl.when(d != me)(copy.wait_send)
+        for which in range(2):
+            pl.when(crosses(s))(p_copy(s, which).wait_send)
+            pl.when(passes(s))(a_copy(s, which).wait_send)
         for which, (src, dst) in enumerate(((mix, mix_in), (stat, stat_in))):
             _, copy = c_copy(s, which, src, dst)
             pl.when(d != me)(copy.wait_send)
@@ -408,8 +469,8 @@
                 b_copy(r, k, att, d_send, d_recv).wait_send()
 
         for_slot(r, drain)
-    for k in range(1, n_tp):
-        e_copy(k).wait_send()
+    for t in range(n_tp):
+        pl.when(tp != t)(e_copy(t).wait_send)
 
 
 def solution(mesh):
@@ -438,7 +499,7 @@
         cols = out_weight.shape[1]
         slots = -(-seqs // n)
         block = rows // n_tp
-        all_w = 3 * width + LANES
+        all_w = 2 * width + LANES
         folded = (2 * props, width // 2)
         vmem = pl.BlockSpec(memory_space=pltpu.VMEM)
         hbm = pl.BlockSpec(memory_space=pl.ANY)
@@ -451,7 +512,11 @@
             out_specs=vmem,
             scratch_shapes=[
                 pltpu.VMEM((seqs, props, all_w), F32),
-                pltpu.VMEM((n - 1, slots, props, all_w), F32),
+                pltpu.VMEM((seqs,) + folded, BF16),
+                pltpu.VMEM((seqs, props, all_w), F32),
+                pltpu.VMEM((seqs,) + folded, BF16),
+                pltpu.VMEM((n // 2 - 1, slots, props, all_w), F32),
+                pltpu.VMEM((n // 2 - 1, slots) + folded, BF16),
                 pltpu.VMEM((depth, gate_weight.shape[1]), BF16),
                 pltpu.VMEM(out_weight.shape, BF16),
                 pltpu.VMEM(cache_keys.shape, BF16),
@@ -472,15 +537,17 @@
                 pltpu.VMEM((-(-seqs // 8) * 8, LANES), jnp.int32),
                 dma((2,)),
                 dma((2, seqs)),
-                dma((seqs,)),
-                dma((n - 1, slots)),
+                dma((2, seqs)),
+                dma((2, seqs)),
+                dma((2, seqs)),
+                dma((2, n // 2 - 1, slots)),
                 dma((slots, n - 1)),
                 dma((seqs,)),
                 dma((2, seqs)),
                 dma((2, n - 1, slots)),
                 dma((slots, n - 1)),
                 dma((seqs,)),
-                dma((n_tp - 1,)),
+                dma((n_tp,)),
                 dma((n_tp - 1,)),
             ],
             compiler_params=pltpu.CompilerParams(

time: 91.8 us -> 77.4 us (0.84)
  Pallas kernels: 80.4 us -> 66.1 us
    pallas_call x1, Pallas kernels: 80.4 us -> 66.1 us  [body(): pl.pallas_call(functools.partial(kernel, n, n_tp), out_shape=jax.ShapeDty...]
where the time goes in v2:
time: 77.4 us; the launch traced here: 76.9 us
  Pallas kernels  66.1 us (85%)
  local copies, waits for them, and re-layouts  10.8 us (14%)
    pallas_call x1, Pallas kernels, body(): pl.pallas_call(functools.partial(kernel, n, n_tp), out_shape=jax.ShapeDty...  66.1 us
    unnamed x22, local copies, waits for them, and re-layouts  10.8 us

profile of v2, /device:TPU:0, one launch (start us, length us, event | category | flops | bytes accessed | tf_op | source)
XLA Modules:
  0.0 76.9 jit_solution(6716129424910512477)
XLA Ops:
  0.0 1.4 %copy.14.gate_hbm = bf16[4096,32]{1,0:T(8,128)(2,1)S(1)} copy(bf16[4096,32]{0,1:T(8,128)(2,1)} %param.18) | data formatting | bytes 524288 | tf_op args[5]
  1.4 0.0 copy-start
  1.4 1.0 %copy-done = bf16[512,512]{1,0:T(8,128)(2,1)S(1)} copy-done((bf16[512,512]{1,0:T(8,128)(2,1)S(1)}, bf16[512,512]{1,0:T(8,128)(2,1)}, u32[]{:S(2)}) %copy-start) | copy-done | bytes 524312
  2.5 0.0 copy-start.1
  2.5 1.0 %copy-done.1 = bf16[512,512]{1,0:T(8,128)(2,1)S(1)} copy-done((bf16[512,512]{1,0:T(8,128)(2,1)S(1)}, bf16[512,512]{1,0:T(8,128)(2,1)}, u32[]{:S(2)}) %copy-start.1) | copy-done | bytes 524312
  3.5 0.0 copy-start.2
  3.5 1.0 %copy-done.2 = bf16[512,512]{1,0:T(8,128)(2,1)S(1)} copy-done((bf16[512,512]{1,0:T(8,128)(2,1)S(1)}, bf16[512,512]{1,0:T(8,128)(2,1)}, u32[]{:S(2)}) %copy-start.2) | copy-done | bytes 524312
  4.6 0.0 copy-start.3
  4.6 1.0 %copy-done.3 = bf16[512,512]{1,0:T(8,128)(2,1)S(1)} copy-done((bf16[512,512]{1,0:T(8,128)(2,1)S(1)}, bf16[512,512]{1,0:T(8,128)(2,1)}, u32[]{:S(2)}) %copy-start.3) | copy-done | bytes 524312
  5.6 0.0 copy-start.4
  5.6 1.0 %copy-done.4 = bf16[288,512]{1,0:T(8,128)(2,1)S(1)} copy-done((bf16[288,512]{1,0:T(8,128)(2,1)S(1)}, bf16[288,512]{1,0:T(8,128)(2,1)}, u32[]{:S(2)}) %copy-start.4) | copy-done | bytes 294936
  6.6 0.0 copy-start.5
  6.6 0.9 %copy-done.5 = f32[12,8,384]{2,1,0:T(8,128)S(1)} copy-done((f32[12,8,384]{2,1,0:T(8,128)S(1)}, f32[12,8,384]{2,1,0:T(8,128)}, u32[]{:S(2)}) %copy-start.5) | copy-done | bytes 147480
  7.5 0.0 copy-start.6
  7.5 0.7 copy-done.6
  8.2 0.0 copy-start.7
  8.2 0.7 copy-done.7
  8.9 0.0 copy-start.8
  8.9 0.7 copy-done.8
  9.5 0.0 copy-start.9
  9.5 0.7 copy-done.9
  10.2 66.1 %shard_map.127 = bf16[72,512]{1,0:T(8,128)(2,1)S(1)} custom-call(bf16[288,512]{1,0:T(8,128)(2,1)S(1)} %copy-done.4, f32[1,512]{1,0:T(1,128)S(1)} %bitcast.2, bf16[512,512]{1,0:T(8,128)(2,1)S(1)} %copy-done, bf16[512,512]{1,0:T(8,128)(2,1)S(1)} %copy-done.1, bf16[512,512]{1,0:T(8,128)(2,1)S(1)} %copy-done.2, bf16[4096,32]{1,0:T(8,128)(2,1)S(1)} %copy.14.gate_hbm, ...), custom_call_target="tpu_custom_call" | custom-call | tf_op jit(solution)/shard_map/pallas_call | solution.py:508
  76.3 0.6 copy.16
Async XLA Ops:
  1.4 1.0 %copy-start = (bf16[512,512]{1,0:T(8,128)(2,1)S(1)}, bf16[512,512]{1,0:T(8,128)(2,1)}, u32[]{:S(2)}) copy-start(bf16[512,512]{1,0:T(8,128)(2,1)} %query_w.1) | copy-start | bytes 1572868
  2.5 1.0 %copy-start.1 = (bf16[512,512]{1,0:T(8,128)(2,1)S(1)}, bf16[512,512]{1,0:T(8,128)(2,1)}, u32[]{:S(2)}) copy-start(bf16[512,512]{1,0:T(8,128)(2,1)} %key_w.1) | copy-start | bytes 1572868
  3.5 1.0 %copy-start.2 = (bf16[512,512]{1,0:T(8,128)(2,1)S(1)}, bf16[512,512]{1,0:T(8,128)(2,1)}, u32[]{:S(2)}) copy-start(bf16[512,512]{1,0:T(8,128)(2,1)} %value_w.1) | copy-start | bytes 1572868
  4.6 1.0 %copy-start.3 = (bf16[512,512]{1,0:T(8,128)(2,1)S(1)}, bf16[512,512]{1,0:T(8,128)(2,1)}, u32[]{:S(2)}) copy-start(bf16[512,512]{1,0:T(8,128)(2,1)} %out_hbm.1) | copy-start | bytes 1572868
  5.6 1.0 %copy-start.4 = (bf16[288,512]{1,0:T(8,128)(2,1)S(1)}, bf16[288,512]{1,0:T(8,128)(2,1)}, u32[]{:S(2)}) copy-start(bf16[288,512]{1,0:T(8,128)(2,1)} %tokens.1) | copy-start | bytes 884740
  6.6 0.9 %copy-start.5 = (f32[12,8,384]{2,1,0:T(8,128)S(1)}, f32[12,8,384]{2,1,0:T(8,128)}, u32[]{:S(2)}) copy-start(f32[12,8,384]{2,1,0:T(8,128)} %decay.1) | copy-start | bytes 442372
  7.5 0.7 copy-start.6
  8.2 0.7 copy-start.7
  8.9 0.7 copy-start.8
  9.5 0.7 copy-start.9
